TPU v7x, 32 devices: a whole 2x2x4 slice. The times are simulated.
32 devices in a mesh: grp: 2 (over x), ep: 8 (over z, y), tp: 2 (over core).
Axes of the slice: x: 2, y: 2, z: 4, core: 2. Of those that a mesh axis runs over, the one named last changes fastest.
Arguments:
- tokens: bfloat16 [4096, 2048], P(('grp', 'ep', 'tp')), parts along dimension 0, may hold values from -6 to 6
- norm_gain: float32 [2048], replicated, may hold values from 0.1 to 1.9
- expert_ids: int32 [4096, 2], P(('grp', 'ep', 'tp')), parts along dimension 0, may hold values from 0 to 7, all different within a row; in each aligned block of 128 rows (0 to 127, 128 to 255, ...) at most 64 rows name the same one
- route_weights: float32 [4096, 2], P(('grp', 'ep', 'tp')), parts along dimension 0, may hold values from 0.2 to 1
- gate_proj: bfloat16 [8, 2048, 1536], P('ep', None, 'tp'), may hold values from -0.375 to 0.375
- linear_proj: bfloat16 [8, 2048, 1536], P('ep', None, 'tp'), may hold values from -0.375 to 0.375
- down_proj: bfloat16 [8, 1536, 2048], P('ep', 'tp'), may hold values from -0.01953125 to 0.01953125
Outputs:
- mixed: bfloat16 [4096, 2048], P(('grp', 'ep', 'tp')), parts along dimension 0
There are 2 independent parts, one for each index of `grp`. A program takes and returns all parts, laid end to end along the dimension named above; an argument that names none is the same for every part. Nothing has to cross between parts.
Inputs may be any that keep to these rules, and one draw needn't show every extreme that they name: `expert_ids`: each token names 2 different experts. Among the 128 rows of one device (aligned blocks) no expert is named more than 64 times, a bound that some expert reaches in some blocks.
All inputs are finite; a program needn't handle non-finite values.
Results may differ from a plain program's by a relative error of at most 0.009.
Values may be sent and summed in bfloat16 or wider, within the bound.
A program may use at most 64 MiB of HBM per device.

v0:
```python
import jax
import jax.numpy as jnp
from jax import lax
from jax.sharding import PartitionSpec as P


def shards(tokens, norm_gain, expert_ids, route_weights, gate_proj, linear_proj, down_proj):
    tok_count, width = tokens.shape
    picks = expert_ids.shape[1]
    experts = lax.axis_size("ep")
    capacity = 2 * tok_count * picks // experts
    values = tokens.astype(jnp.float32)
    normed = (
        values * lax.rsqrt(jnp.mean(values * values, axis=-1, keepdims=True) + 1e-06) * norm_gain
    ).astype(jnp.bfloat16)
    flat = expert_ids.reshape(-1)
    onehot = (flat[:, None] == jnp.arange(experts, dtype=jnp.int32)[None, :]).astype(jnp.int32)
    slots = jnp.sum((jnp.cumsum(onehot, axis=0) - 1) * onehot, axis=1)
    where = flat * capacity + slots
    buffer = (
        jnp.zeros((experts * capacity, width), jnp.bfloat16)
        .at[where]
        .set(jnp.repeat(normed, picks, axis=0))
    )
    arrived = lax.all_to_all(buffer, "ep", split_axis=0, concat_axis=0, tiled=True)
    rows = lax.all_gather(arrived, "tp", axis=0, tiled=True)
    gate_pre = jnp.dot(rows, gate_proj[0], preferred_element_type=jnp.float32)
    lin_pre = jnp.dot(rows, linear_proj[0], preferred_element_type=jnp.float32)
    glu = jnp.minimum(gate_pre, 7.0)
    lin = jnp.clip(lin_pre, -7.0, 7.0)
    hidden = (glu * jax.nn.sigmoid(1.702 * glu) * (lin + 1.0)).astype(jnp.bfloat16)
    rows = hidden
    summed = lax.psum_scatter(
        jnp.dot(rows, down_proj[0], preferred_element_type=jnp.float32).astype(jnp.bfloat16),
        "tp",
        scatter_dimension=0,
        tiled=True,
    )
    returned = lax.all_to_all(summed, "ep", split_axis=0, concat_axis=0, tiled=True)
    picked = returned[where].reshape(tok_count, picks, width).astype(jnp.float32)
    return jnp.sum(picked * route_weights[:, :, None], axis=1).astype(jnp.bfloat16)


def solution(mesh):
    placed = (
        P(("grp", "ep", "tp"), None),
        P(),
        P(("grp", "ep", "tp"), None),
        P(("grp", "ep", "tp"), None),
        P("ep", None, "tp"),
        P("ep", None, "tp"),
        P("ep", "tp", None),
    )
    return jax.shard_map(
        shards, mesh=mesh, in_specs=placed, out_specs=P(("grp", "ep", "tp"), None), check_vma=False
    )
```

profile of v0, /device:TPU:24, one launch (start us, length us, event | category | flops | bytes accessed | tf_op | source)
XLA Modules:
  0.0 195.9 jit_solution(6481131726988082213)
XLA Ops:
  6.5 0.0 copy-start
  6.5 0.0 all-gather.2.cloned.1.call-start
  6.5 0.9 copy.10
  7.5 0.1 eq.29
  7.6 0.1 eq.25
  7.8 0.7 broadcast_multiply_fusion
  8.4 0.6 reduce-window.6
  9.0 0.2 slice_reduce_fusion
  9.3 0.1 copy.9
  9.4 0.1 mul.60
  9.5 1.2 fusion.7
  10.8 1.2 fusion.9
  12.0 1.6 broadcast_in_dim.5
  13.6 2.3 %reshape.83 = bf16[256,2048]{1,0:T(8,128)(2,1)} reshape(bf16[128,2,2048]{2,1,0:T(2,128)(2,1)} %broadcast_in_dim.5) | data formatting | bytes 2097152 | tf_op jit(solution)/shard_map/reshape | solution.py:23
  15.9 0.1 fusion.14
  16.0 4.4 %scatter_custom_fusion = bf16[512,2048]{1,0:T(8,128)(2,1)} fusion(s32[256]{0:T(256)S(1)} %bitcast.30, bf16[256,2048]{1,0:T(8,128)(2,1)} %reshape.83, bf16[]{:T(256)} %constant.12.clone.1), kind=kCustom, calls=%fused_computation.15 | custom fusion | bytes 2097664 | tf_op jit(solution)/shard_map/scatter | solution.py:23
  20.4 51.7 %all_to_all.24 = bf16[8,64,2048]{2,1,0:T(8,128)(2,1)} all-to-all(bf16[8,64,2048]{2,1,0:T(8,128)(2,1)} %bitcast.28), channel_id=1, replica_groups=mesh['grp'=2,'ep'=8,'tp'=2] {'ep'}, dimensions={0} | all-to-all | bytes 4194304 | tf_op jit(solution)/shard_map/all_to_all | solution.py:25
  72.1 0.0 all-gather.2.cloned.1.call-update
  72.2 0.0 reduce-scatter.2.cloned.1.call-start
  72.2 15.2 %all-gather.2.cloned.1.call-done = bf16[1024,2048]{1,0:T(8,128)(2,1)} async-done(((bf16[512,2048]{1,0:T(8,128)(2,1)}), bf16[1024,2048]{1,0:T(8,128)(2,1)}) %all-gather.2.cloned.1.call-update) | async-done | bytes 4194320 | tf_op jit(solution)/shard_map/all_gather | solution.py:26
  87.4 8.3 %fusion.1 = f32[1024,768]{1,0:T(8,128)} fusion(bf16[1024,2048]{1,0:T(8,128)(2,1)} %all-gather.2.cloned.1.call-done, bf16[1,2048,768]{2,1,0:T(8,128)(2,1)} %param.12), kind=kOutput, calls=%fused_computation.4 | convolution fusion | flops 3221225472 | bytes 10485760 | tf_op jit(solution)/shard_map/dot_general | solution.py:28
  95.8 0.0 copy-done
  95.8 12.5 %convolution_convert_fusion = bf16[1024,2048]{1,0:T(8,128)(2,1)} fusion(bf16[1,768,2048]{2,1,0:T(8,128)(2,1)S(1)} %copy-done, f32[1024,768]{1,0:T(8,128)} %fusion.1, bf16[1024,2048]{1,0:T(8,128)(2,1)} %all-gather.2.cloned.1.call-done, bf16[1,2048,768]{2,1,0:T(8,128)(2,1)} %param.11), kind=kOutput, calls=%fused_computation.2 | convolution fusion | flops 6452412416 | bytes 17825792 | tf_op jit(solution)/shard_map/dot_general | solution.py:34
  108.3 0.0 reduce-scatter.2.cloned.1.call-update
  108.3 0.0 copy-start.1
  108.3 13.5 %reduce-scatter.2.cloned.1.call-done = bf16[512,2048]{1,0:T(8,128)(2,1)} async-done(((bf16[1024,2048]{1,0:T(8,128)(2,1)}), bf16[512,2048]{1,0:T(8,128)(2,1)}) %reduce-scatter.2.cloned.1.call-update) | async-done | bytes 2097168 | tf_op jit(solution)/shard_map/reduce_scatter | solution.py:33
  121.8 6.0 %all-to-all-start.1 = ((bf16[8,64,2048]{2,1,0:T(8,128)(2,1)}), bf16[8,64,2048]{2,1,0:T(8,128)(2,1)}, u32[]{:S(2)}, u32[]{:S(2)}) async-start(bf16[8,64,2048]{2,1,0:T(8,128)(2,1)} %bitcast.29), calls=%async_computation.2 | async-start | bytes 4194304 | tf_op jit(solution)/shard_map/all_to_all | solution.py:39
  127.8 0.0 copy-done.1
  127.8 0.1 copy.12
  127.9 47.0 %all-to-all-done.1 = bf16[8,64,2048]{2,1,0:T(8,128)(2,1)} async-done(((bf16[8,64,2048]{2,1,0:T(8,128)(2,1)}), bf16[8,64,2048]{2,1,0:T(8,128)(2,1)}, u32[]{:S(2)}, u32[]{:S(2)}) %all-to-all-start.1) | async-done | bytes 2097184 | tf_op jit(solution)/shard_map/all_to_all | solution.py:39
  174.9 5.2 %gather_fusion = bf16[256,2048]{1,0:T(8,128)(2,1)} fusion(bf16[512,2048]{1,0:T(8,128)(2,1)} %bitcast.10, s32[1024]{0:T(1024)S(1)} %pad_clamp_fusion), kind=kCustom, calls=%fused_computation | custom fusion | bytes 2098176 | tf_op jit(solution)/shard_map/gather | solution.py:40
  180.1 3.4 %reshape.70 = f32[128,2,2048]{2,1,0:T(2,128)} reshape(bf16[256,2048]{1,0:T(8,128)(2,1)} %gather_fusion) | data formatting | bytes 3145728 | tf_op jit(solution)/shard_map/convert_element_type | solution.py:40
  183.5 5.6 %multiply_reduce_fusion = bf16[128,2048]{1,0:T(8,128)(2,1)} fusion(f32[128,2,2048]{2,1,0:T(2,128)} %reshape.70, f32[128,2]{1,0:T(8,128)S(1)} %copy.12), kind=kLoop, calls=%fused_computation.9 | loop fusion | flops 786432 | bytes 2622464 | tf_op jit(solution)/shard_map/reduce_sum | solution.py:41
  (6 shorter events, 0.1 us)
Async XLA Ops:
  6.5 89.2 %copy-start = (bf16[1,768,2048]{2,1,0:T(8,128)(2,1)S(1)}, bf16[1,768,2048]{2,1,0:T(8,128)(2,1)}, u32[]{:S(2)}) copy-start(bf16[1,768,2048]{2,1,0:T(8,128)(2,1)} %param.13) | copy-start | bytes 9437188
  6.5 80.9 %all-gather.2.cloned.1.call-start = ((), (), s32[]{:S(2)}) async-start(), calls=%async_computation.3 | async-start | bytes 6291456 | tf_op jit(solution)/shard_map/all_gather | solution.py:26
  72.2 49.6 %reduce-scatter.2.cloned.1.call-start = ((), (), s32[]{:S(2)}) async-start(), calls=%async_computation.4 | async-start | bytes 6291456 | tf_op jit(solution)/shard_map/reduce_scatter | solution.py:33
  108.3 19.5 %copy-start.1 = (f32[128,2]{0,1:T(2,128)S(1)}, f32[128,2]{0,1:T(2,128)}, u32[]{:S(2)}) copy-start(f32[128,2]{0,1:T(2,128)} %param.10) | copy-start | bytes 3076
  121.8 53.1 %all-to-all-start.1 = ((bf16[8,64,2048]{2,1,0:T(8,128)(2,1)}), bf16[8,64,2048]{2,1,0:T(8,128)(2,1)}, u32[]{:S(2)}, u32[]{:S(2)}) async-start(bf16[8,64,2048]{2,1,0:T(8,128)(2,1)} %bitcast.29), calls=%async_computation.2 | async-start | bytes 4194304 | tf_op jit(solution)/shard_map/all_to_all | solution.py:39
Sparse Core Ops, SparseCore 0:
  72.3 15.1 all-gather.1
  108.4 13.3 reduce-scatter.1
where the time goes:
time: 199 us; the launch traced here: 196 us
  waiting for transfers between devices  75.8 us (38%)
  blocking collectives  51.7 us (26%)
  matrix products  20.8 us (10%)
  local copies, waits for them, and re-layouts  18.7 us (9%)
  between operations  13.4 us (7%)
  other arithmetic  9.46 us (5%)
  starting transfers between devices  6.03 us (3%)
    all_to_all x1, blocking collectives, shards(): lax.all_to_all(buffer, 'ep', split_axis=0, concat_axis=0, tiled=True)  51.7 us
    all_to_all x1, waiting for transfers between devices, shards(): lax.all_to_all(summed, 'ep', split_axis=0, concat_axis=0, tiled=True)  47 us
    all_gather x1, waiting for transfers between devices, shards(): rows = lax.all_gather(arrived, 'tp', axis=0, tiled=True)  15.2 us
    reduce_scatter x1, waiting for transfers between devices, shards(): lax.psum_scatter(jnp.dot(rows, down_proj[0], preferred_element_type=jnp.f...  13.5 us
    dot_general x1, matrix products, shards(): jnp.dot(rows, down_proj[0], preferred_element_type=jnp.float32)  12.5 us
    dot_general x1, matrix products, shards(): lin_pre = jnp.dot(rows, linear_proj[0], preferred_element_type=jnp.float32)  8.33 us
    all_to_all x1, starting transfers between devices, shards(): lax.all_to_all(summed, 'ep', split_axis=0, concat_axis=0, tiled=True)  5.99 us
    reduce_sum x1, other arithmetic, shards(): jnp.sum(picked * route_weights[:, :, None], axis=1).astype(jnp.bfloat16)  5.59 us
  transfers between devices with their start and end apart: 3, of which 3 were waited for; matrix products, arithmetic and copies ran while one was open for 0% of the time, Pallas kernels for 0%

commit v1 on v0

--- a/solution.py
+++ b/solution.py
@@ -1,7 +1,13 @@
+import functools
+
 import jax
 import jax.numpy as jnp
 from jax import lax
+from jax.experimental import pallas as pl
+from jax.experimental.pallas import tpu as pltpu
 from jax.sharding import PartitionSpec as P
+
+MESH = pl.DeviceIdType.MESH
 
 
 def shards(tokens, norm_gain, expert_ids, route_weights, gate_proj, linear_proj, down_proj):
@@ -41,6 +47,311 @@
     return jnp.sum(picked * route_weights[:, :, None], axis=1).astype(jnp.bfloat16)
 
 
+def kernel(
+    line, ids_ref, weights_ref, gain_ref, tokens_ref, gate_hbm, linear_hbm, down_hbm, out_ref,
+    gate, linear, down, tok, meta, rows, cross, hidden, part, part_in, done, done_in, back, back_in,
+    load_sem, tok_send, tok_recv, meta_send, meta_recv, cross_send, cross_recv, pair_send, pair_recv,
+    part_send, part_recv, done_send, done_recv, back_send, back_recv,
+):
+    ep, core = lax.axis_index("ep"), lax.axis_index("tp")
+    z, y = ep // 2, ep % 2
+    experts = 2 * line
+    tok_count, width = tokens_ref.shape
+    capacity = rows.shape[3]
+    ff = gate.shape[1]
+    at_y = {"ep": z * 2 + 1 - y}
+    at_core = {"tp": 1 - core}
+
+    def at_z(other):
+        return {"ep": other * 2 + y}
+
+    def remote(source, target, send, recv, device):
+        return pltpu.make_async_remote_copy(
+            src_ref=source, dst_ref=target, send_sem=send, recv_sem=recv,
+            device_id=device, device_id_type=MESH,
+        )
+
+    loads = [
+        pltpu.make_async_copy(source, target, load_sem.at[i])
+        for i, (source, target) in enumerate(((gate_hbm, gate), (linear_hbm, linear), (down_hbm, down)))
+    ]
+    for load in loads:
+        load.start()
+    barrier = pltpu.get_barrier_semaphore()
+    for step in range(1, line):
+        pl.semaphore_signal(barrier, 1, device_id=at_z((z + step) % line), device_id_type=MESH)
+    pl.semaphore_signal(barrier, 1, device_id=at_y, device_id_type=MESH)
+    pl.semaphore_signal(barrier, 1, device_id=at_core, device_id_type=MESH)
+
+    def normalize(i, _):
+        span = pl.ds(pl.multiple_of(i * 32, 32), 32)
+        values = tokens_ref[span, :].astype(jnp.float32)
+        scale = lax.rsqrt(jnp.mean(values * values, axis=-1, keepdims=True) + 1e-06)
+        tok[z, span, :] = (values * scale * gain_ref[...]).astype(jnp.bfloat16)
+        return 0
+
+    lax.fori_loop(0, tok_count // 32, normalize, 0)
+    names = lax.broadcasted_iota(jnp.int32, (experts, tok_count), 0)
+    share = jnp.zeros((experts, tok_count), jnp.float32)
+    chosen = jnp.zeros((experts, tok_count), jnp.float32)
+    for pick in range(ids_ref.shape[0]):
+        same = ids_ref[pick : pick + 1, :] == names
+        share = share + jnp.where(same, weights_ref[pick : pick + 1, :], 0.0)
+        chosen = chosen + jnp.where(same, 1.0, 0.0)
+    first = lax.broadcasted_iota(jnp.int32, (tok_count, tok_count), 0)
+    second = lax.broadcasted_iota(jnp.int32, (tok_count, tok_count), 1)
+    eye = first == second
+    before = jnp.where(first < second, 1.0, 0.0).astype(jnp.bfloat16)
+    slots = jnp.dot(chosen.astype(jnp.bfloat16), before, preferred_element_type=jnp.float32)
+    meta[z, 0:experts, :] = jnp.where(chosen > 0.5, slots, -1.0)
+    meta[z, experts : 2 * experts, :] = share
+    pl.semaphore_wait(barrier, line + 1)
+
+    def meta_copy(step):
+        return remote(meta.at[z], meta.at[z], meta_send.at[step], meta_recv.at[z], at_z((z + step) % line))
+
+    def meta_arrival(source):
+        return remote(meta.at[source], meta.at[source], meta_send.at[0], meta_recv.at[source], at_z((z + 1) % line))
+
+    for step in range(1, line):
+        meta_copy(step).start()
+
+    def order(step):
+        found = z
+        for place in range(line):
+            nearest = sorted(range(line), key=lambda other: (abs(other - place), other))
+            found = jnp.where(z == place, nearest[step], found)
+        return found if step else z
+
+    def hop(source, side):
+        return remote(
+            tok.at[source], tok.at[source], tok_send.at[source, side], tok_recv.at[source],
+            at_z(lax.rem(z + (1 if side else line - 1), line)),
+        )
+
+    def hops(source, act):
+        @pl.when((source <= z) & (z < line - 1))
+        def _():
+            act(hop(source, 1))
+
+        @pl.when((source >= z) & (z > 0))
+        def _():
+            act(hop(source, 0))
+
+    def cross_copy(source):
+        return remote(cross.at[source], rows.at[source, core, y], cross_send.at[source], cross_recv.at[source], at_y)
+
+    def cross_arrival(source):
+        return remote(cross.at[source], rows.at[source, core, 1 - y], cross_send.at[source], cross_recv.at[source], at_y)
+
+    def pair_copy(source, column):
+        block = rows.at[source, core, column]
+        return remote(block, block, pair_send.at[source, column], pair_recv.at[source, column], at_core)
+
+    def pair_arrival(source, column):
+        block = rows.at[source, 1 - core, column]
+        return remote(block, block, pair_send.at[source, column], pair_recv.at[source, column], at_core)
+
+    def part_copy(source):
+        return remote(part.at[source, 1 - core], part_in.at[source], part_send.at[source], part_recv.at[source], at_core)
+
+    def done_copy(source):
+        return remote(done.at[source, 1 - y], done_in.at[source], done_send.at[source], done_recv.at[source], at_y)
+
+    def back_copy(source):
+        return remote(back.at[source], back_in.at[z], back_send.at[source], back_recv.at[z], at_z(source))
+
+    def back_arrival(source):
+        return remote(back.at[source], back_in.at[source], back_send.at[source], back_recv.at[source], at_z(source))
+
+    tile = 512
+
+    def over_width(act):
+        def go(i, _):
+            act(pl.ds(pl.multiple_of(i * tile, tile), tile))
+            return 0
+
+        lax.fori_loop(0, width // tile, go, 0)
+
+    def dispatch(step):
+        source = order(step)
+        if step:
+            hop(source, 0).wait_recv()
+        hops(source, lambda copy: copy.start())
+        if step:
+            meta_arrival(source).wait_recv()
+        place = lax.broadcasted_iota(jnp.int32, (capacity, tok_count), 0).astype(jnp.float32)
+        away = (meta[source, pl.ds(z * 2 + 1 - y, 1), :] == place).astype(jnp.bfloat16)
+        here = (meta[source, pl.ds(z * 2 + y, 1), :] == place).astype(jnp.bfloat16)
+
+        def send_away(span):
+            cross[source, :, span] = jnp.dot(
+                away, tok[source, :, span], preferred_element_type=jnp.float32
+            ).astype(jnp.bfloat16)
+
+        def keep_here(span):
+            rows[source, core, y, :, span] = jnp.dot(
+                here, tok[source, :, span], preferred_element_type=jnp.float32
+            ).astype(jnp.bfloat16)
+
+        over_width(send_away)
+        cross_copy(source).start()
+        over_width(keep_here)
+        pair_copy(source, y).start()
+
+    def forward(step):
+        source = order(step)
+        cross_arrival(source).wait_recv()
+        pair_copy(source, 1 - y).start()
+
+    def compute(step):
+        source = order(step)
+        for column in range(2):
+            pair_arrival(source, column).wait_recv()
+        if step == 0:
+            loads[0].wait()
+            loads[1].wait()
+        depth = 256
+
+        def up(i, _):
+            span = pl.ds(pl.multiple_of(i * depth, depth), depth)
+            block = rows[source].reshape(4 * capacity, width)
+            glu = jnp.minimum(jnp.dot(block, gate[:, span], preferred_element_type=jnp.float32), 7.0)
+            lin = jnp.clip(jnp.dot(block, linear[:, span], preferred_element_type=jnp.float32), -7.0, 7.0)
+            hidden[:, span] = (glu * jax.nn.sigmoid(1.702 * glu) * (lin + 1.0)).astype(jnp.bfloat16)
+            return 0
+
+        lax.fori_loop(0, ff // depth, up, 0)
+        if step == 0:
+            loads[2].wait()
+
+        def out(span):
+            part[source, :, :, :, span] = (
+                jnp.dot(hidden[...], down[:, span], preferred_element_type=jnp.float32)
+                .astype(jnp.bfloat16)
+                .reshape(2, 2, capacity, tile)
+            )
+
+        over_width(out)
+        part_copy(source).start()
+
+    def finish(step):
+        source = order(step)
+        part_copy(source).wait_recv()
+
+        def add(span):
+            total = part[source, core, :, :, span].astype(jnp.float32) + part_in[source, :, :, span].astype(
+                jnp.float32
+            )
+            done[source, :, :, span] = total.astype(jnp.bfloat16)
+
+        over_width(add)
+        done_copy(source).start()
+
+    def combine(step):
+        source = order(step)
+        done_copy(source).wait_recv()
+        lane = lax.broadcasted_iota(jnp.int32, (tok_count, capacity), 1).astype(jnp.float32)
+
+        def column(row):
+            return jnp.sum(jnp.where(eye, meta[source, pl.ds(row, 1), :], 0.0), axis=1, keepdims=True)
+
+        mine, other = z * 2 + y, z * 2 + 1 - y
+        spread_mine = (column(mine) == lane).astype(jnp.bfloat16)
+        spread_other = (column(other) == lane).astype(jnp.bfloat16)
+        share_mine, share_other = column(experts + mine), column(experts + other)
+
+        def merge(span):
+            total = share_mine * jnp.dot(
+                spread_mine, done[source, y, :, span], preferred_element_type=jnp.float32
+            ) + share_other * jnp.dot(spread_other, done_in[source, :, span], preferred_element_type=jnp.float32)
+            back[source, :, span] = total.astype(jnp.bfloat16)
+
+        over_width(merge)
+        if step:
+            back_copy(source).start()
+
+    for tick in range(line + 2):
+        if tick < line:
+            dispatch(tick)
+        if 0 <= tick - 1 < line:
+            compute(tick - 1)
+        if tick < line:
+            forward(tick)
+        if 0 <= tick - 1 < line:
+            finish(tick - 1)
+        if 0 <= tick - 2 < line:
+            combine(tick - 2)
+    for step in range(1, line):
+        back_arrival(order(step)).wait_recv()
+
+    def gather(span):
+        total = back[z, :, span].astype(jnp.float32)
+        for step in range(1, line):
+            total = total + back_in[order(step), :, span].astype(jnp.float32)
+        out_ref[:, span] = total.astype(jnp.bfloat16)
+
+    over_width(gather)
+    for step in range(line):
+        source = order(step)
+        hops(source, lambda copy: copy.wait_send())
+        if step:
+            meta_copy(step).wait_send()
+            back_copy(source).wait_send()
+        cross_copy(source).wait_send()
+        for column in range(2):
+            pair_copy(source, column).wait_send()
+        part_copy(source).wait_send()
+        done_copy(source).wait_send()
+
+
+def fused(line, tokens, norm_gain, expert_ids, route_weights, gate_proj, linear_proj, down_proj):
+    tok_count, width = tokens.shape
+    picks = expert_ids.shape[1]
+    experts = 2 * line
+    capacity = 2 * tok_count * picks // experts
+    ff = gate_proj.shape[2]
+    wide, dma = jnp.bfloat16, pltpu.SemaphoreType.DMA
+    inside, outside = pl.BlockSpec(memory_space=pltpu.VMEM), pl.BlockSpec(memory_space=pl.ANY)
+    return pl.pallas_call(
+        functools.partial(kernel, line),
+        out_shape=jax.ShapeDtypeStruct((tok_count, width), wide),
+        in_specs=[inside] * 4 + [outside] * 3,
+        out_specs=inside,
+        scratch_shapes=[
+            pltpu.VMEM((width, ff), wide),
+            pltpu.VMEM((width, ff), wide),
+            pltpu.VMEM((ff, width), wide),
+            pltpu.VMEM((line, tok_count, width), wide),
+            pltpu.VMEM((line, 2 * experts, tok_count), jnp.float32),
+            pltpu.VMEM((line, 2, 2, capacity, width), wide),
+            pltpu.VMEM((line, capacity, width), wide),
+            pltpu.VMEM((4 * capacity, ff), wide),
+            pltpu.VMEM((line, 2, 2, capacity, width), wide),
+            pltpu.VMEM((line, 2, capacity, width), wide),
+            pltpu.VMEM((line, 2, capacity, width), wide),
+            pltpu.VMEM((line, capacity, width), wide),
+            pltpu.VMEM((line, tok_count, width), wide),
+            pltpu.VMEM((line, tok_count, width), wide),
+            dma((3,)),
+            dma((line, 2)), dma((line,)),
+            dma((line,)), dma((line,)),
+            dma((line,)), dma((line,)),
+            dma((line, 2)), dma((line, 2)),
+            dma((line,)), dma((line,)),
+            dma((line,)), dma((line,)),
+            dma((line,)), dma((line,)),
+        ],
+        compiler_params=pltpu.CompilerParams(
+            collective_id=0, has_side_effects=True, vmem_limit_bytes=60 * 1024 * 1024
+        ),
+        name="experts",
+    )(
+        expert_ids.T, route_weights.T, norm_gain.reshape(1, width), tokens,
+        gate_proj[0], linear_proj[0], down_proj[0],
+    )
+
+
 def solution(mesh):
     placed = (
         P(("grp", "ep", "tp"), None),
@@ -51,6 +362,13 @@
         P("ep", None, "tp"),
         P("ep", "tp", None),
     )
+    along = [device.coords[2] for device in mesh.devices[0, :, 0]]
+    line = len(set(along))
+    paired = line > 1 and along == [index // 2 for index in range(2 * line)] and mesh.shape["tp"] == 2
     return jax.shard_map(
-        shards, mesh=mesh, in_specs=placed, out_specs=P(("grp", "ep", "tp"), None), check_vma=False
-    )
+        functools.partial(fused, line) if paired else shards,
+        mesh=mesh,
+        in_specs=placed,
+        out_specs=P(("grp", "ep", "tp"), None),
+        check_vma=False,
+    )

time: 199 us -> 109 us (0.55)
  Pallas kernels: 0 us -> 105 us
  waiting for transfers between devices: 75.8 us -> 0 us
  blocking collectives: 51.7 us -> 0 us
  matrix products: 20.8 us -> 0 us
  local copies, waits for them, and re-layouts: 18.7 us -> 1.88 us
  between operations: 13.4 us -> 0.01 us
  other arithmetic: 9.46 us -> 0 us
  starting transfers between devices: 6.03 us -> 0 us
    pallas_call x0 -> x1, Pallas kernels: none -> 105 us  [fused(): pl.pallas_call(functools.partial(kernel, line), out_shape=jax.ShapeDtypeS...]
    all_to_all x1 -> x0, blocking collectives: 51.7 us -> none  [shards(): lax.all_to_all(buffer, 'ep', split_axis=0, concat_axis=0, tiled=True)]
    all_to_all x1 -> x0, waiting for transfers between devices: 47 us -> none  [shards(): lax.all_to_all(summed, 'ep', split_axis=0, concat_axis=0, tiled=True)]
    dot_general x2 -> x0, matrix products: 20.8 us -> none  [the longest x1 12.5 us: shards(): jnp.dot(rows, down_proj[0], preferred_element_type=jnp.float32)]
    all_gather x1 -> x0, waiting for transfers between devices: 15.2 us -> none  [shards(): rows = lax.all_gather(arrived, 'tp', axis=0, tiled=True)]
    reduce_scatter x1 -> x0, waiting for transfers between devices: 13.5 us -> none  [shards(): lax.psum_scatter(jnp.dot(rows, down_proj[0], preferred_element_type=jnp.f...]
    reduce_sum x3 -> x0, other arithmetic: 6.9 us -> none  [the longest x1 5.59 us: shards(): jnp.sum(picked * route_weights[:, :, None], axis=1).astype(jnp.bfloat16)]
    all_to_all x1 -> x0, starting transfers between devices: 5.99 us -> none  [shards(): lax.all_to_all(summed, 'ep', split_axis=0, concat_axis=0, tiled=True)]
  transfers between devices with their start and end apart: 3 -> 0, of which waited for: 3 -> 0; matrix products, arithmetic and copies ran while one was open for 0% -> 0% of each run, Pallas kernels for 0% -> 0%
where the time goes in v1:
time: 109 us; the launch traced here: 107 us
  Pallas kernels  105 us (96%)
  local copies, waits for them, and re-layouts  1.88 us (2%)
    pallas_call x1, Pallas kernels, fused(): pl.pallas_call(functools.partial(kernel, line), out_shape=jax.ShapeDtypeS...  105 us

profile of v1, /device:TPU:24, one launch (start us, length us, event | category | flops | bytes accessed | tf_op | source)
XLA Modules:
  0.0 107.1 jit_solution(17878386474007528409)
XLA Ops:
  0.0 105.2 %experts.1 = bf16[128,2048]{1,0:T(8,128)(2,1)} custom-call(s32[2,128]{1,0:T(2,128)} %bitcast.10, f32[2,128]{1,0:T(2,128)} %bitcast.11, f32[1,2048]{1,0:T(1,128)} %bitcast.9, bf16[128,2048]{1,0:T(8,128)(2,1)} %tokens_ref.1, bf16[2048,768]{1,0:T(8,128)(2,1)} %bitcast.6, bf16[2048,768]{1,0:T(8,128)(2,1)} %bitcast.7, bf16[768,2048]{1,0:T(8,128)(2,1)} %bitcast.8), custom_call_target="tpu_custom_call" | custom-call | tf_op jit(solution)/shard_map/experts/pallas_call | solution.py:316
  105.2 1.9 %copy.9 = bf16[128,2048]{1,0:T(8,128)(2,1)} copy(bf16[128,2048]{1,0:T(8,128)(2,1)} %experts.1) | data formatting | bytes 1048576

commit v2 on v1

--- a/solution.py
+++ b/solution.py
@@ -8,6 +8,7 @@
 from jax.sharding import PartitionSpec as P
 
 MESH = pl.DeviceIdType.MESH
+PARTS = 2
 
 
 def shards(tokens, norm_gain, expert_ids, route_weights, gate_proj, linear_proj, down_proj):
@@ -59,6 +60,8 @@
     tok_count, width = tokens_ref.shape
     capacity = rows.shape[3]
     ff = gate.shape[1]
+    half = width // PARTS
+    cols = [slice(i * half, (i + 1) * half) for i in range(PARTS)]
     at_y = {"ep": z * 2 + 1 - y}
     at_core = {"tp": 1 - core}
 
@@ -123,64 +126,88 @@
             found = jnp.where(z == place, nearest[step], found)
         return found if step else z
 
-    def hop(source, side):
-        return remote(
-            tok.at[source], tok.at[source], tok_send.at[source, side], tok_recv.at[source],
+    def hop(source, i, side):
+        block = tok.at[source, :, cols[i]]
+        return remote(
+            block, block, tok_send.at[source, i, side], tok_recv.at[source, i],
             at_z(lax.rem(z + (1 if side else line - 1), line)),
         )
 
-    def hops(source, act):
+    def hops(source, i, act):
         @pl.when((source <= z) & (z < line - 1))
         def _():
-            act(hop(source, 1))
+            act(hop(source, i, 1))
 
         @pl.when((source >= z) & (z > 0))
         def _():
-            act(hop(source, 0))
-
-    def cross_copy(source):
-        return remote(cross.at[source], rows.at[source, core, y], cross_send.at[source], cross_recv.at[source], at_y)
-
-    def cross_arrival(source):
-        return remote(cross.at[source], rows.at[source, core, 1 - y], cross_send.at[source], cross_recv.at[source], at_y)
-
-    def pair_copy(source, column):
-        block = rows.at[source, core, column]
-        return remote(block, block, pair_send.at[source, column], pair_recv.at[source, column], at_core)
-
-    def pair_arrival(source, column):
-        block = rows.at[source, 1 - core, column]
-        return remote(block, block, pair_send.at[source, column], pair_recv.at[source, column], at_core)
-
-    def part_copy(source):
-        return remote(part.at[source, 1 - core], part_in.at[source], part_send.at[source], part_recv.at[source], at_core)
-
-    def done_copy(source):
-        return remote(done.at[source, 1 - y], done_in.at[source], done_send.at[source], done_recv.at[source], at_y)
-
-    def back_copy(source):
-        return remote(back.at[source], back_in.at[z], back_send.at[source], back_recv.at[z], at_z(source))
-
-    def back_arrival(source):
-        return remote(back.at[source], back_in.at[source], back_send.at[source], back_recv.at[source], at_z(source))
+            act(hop(source, i, 0))
+
+    def cross_copy(source, i):
+        return remote(
+            cross.at[source, :, cols[i]], rows.at[source, core, y, :, cols[i]],
+            cross_send.at[source, i], cross_recv.at[source, i], at_y,
+        )
+
+    def cross_arrival(source, i):
+        return remote(
+            cross.at[source, :, cols[i]], rows.at[source, core, 1 - y, :, cols[i]],
+            cross_send.at[source, i], cross_recv.at[source, i], at_y,
+        )
+
+    def pair_move(source, owner, column, i):
+        block = rows.at[source, owner, column, :, cols[i]]
+        return remote(block, block, pair_send.at[source, column, i], pair_recv.at[source, column, i], at_core)
+
+    def part_copy(source, i):
+        return remote(
+            part.at[source, 1 - core, :, :, cols[i]], part_in.at[source, :, :, cols[i]],
+            part_send.at[source, i], part_recv.at[source, i], at_core,
+        )
+
+    def done_copy(source, i):
+        return remote(
+            done.at[source, 1 - y, :, cols[i]], done_in.at[source, :, cols[i]],
+            done_send.at[source, i], done_recv.at[source, i], at_y,
+        )
+
+    def back_copy(source, i):
+        return remote(
+            back.at[source, :, cols[i]], back_in.at[z, :, cols[i]],
+            back_send.at[source, i], back_recv.at[z, i], at_z(source),
+        )
+
+    def back_arrival(source, i):
+        return remote(
+            back.at[source, :, cols[i]], back_in.at[source, :, cols[i]],
+            back_send.at[source, i], back_recv.at[source, i], at_z(source),
+        )
 
     tile = 512
 
-    def over_width(act):
-        def go(i, _):
-            act(pl.ds(pl.multiple_of(i * tile, tile), tile))
+    def over_width(i, act):
+        def go(j, _):
+            act(pl.ds(pl.multiple_of(i * half + j * tile, tile), tile))
             return 0
 
-        lax.fori_loop(0, width // tile, go, 0)
+        lax.fori_loop(0, half // tile, go, 0)
+
+    def arrive(tick, i):
+        if tick == 0:
+            hops(z, i, lambda copy: copy.start())
+        for step in range(max(tick, 1), line):
+            source = order(step)
+            apart = jnp.where(source > z, source - z, z - source)
+
+            @pl.when(apart == tick)
+            def _():
+                hop(source, i, 0).wait_recv()
+                hops(source, i, lambda copy: copy.start())
 
     def dispatch(step):
         source = order(step)
-        if step:
-            hop(source, 0).wait_recv()
-        hops(source, lambda copy: copy.start())
+        place = lax.broadcasted_iota(jnp.int32, (capacity, tok_count), 0).astype(jnp.float32)
         if step:
             meta_arrival(source).wait_recv()
-        place = lax.broadcasted_iota(jnp.int32, (capacity, tok_count), 0).astype(jnp.float32)
         away = (meta[source, pl.ds(z * 2 + 1 - y, 1), :] == place).astype(jnp.bfloat16)
         here = (meta[source, pl.ds(z * 2 + y, 1), :] == place).astype(jnp.bfloat16)
 
@@ -194,20 +221,28 @@
                 here, tok[source, :, span], preferred_element_type=jnp.float32
             ).astype(jnp.bfloat16)
 
-        over_width(send_away)
-        cross_copy(source).start()
-        over_width(keep_here)
-        pair_copy(source, y).start()
+        if step == 0:
+            for i in range(PARTS):
+                arrive(step, i)
+        for i in range(PARTS):
+            if step:
+                arrive(step, i)
+            over_width(i, send_away)
+            cross_copy(source, i).start()
+            over_width(i, keep_here)
+            pair_move(source, core, y, i).start()
 
     def forward(step):
         source = order(step)
-        cross_arrival(source).wait_recv()
-        pair_copy(source, 1 - y).start()
+        for i in range(PARTS):
+            cross_arrival(source, i).wait_recv()
+            pair_move(source, core, 1 - y, i).start()
 
     def compute(step):
         source = order(step)
         for column in range(2):
-            pair_arrival(source, column).wait_recv()
+            for i in range(PARTS):
+                pair_move(source, 1 - core, column, i).wait_recv()
         if step == 0:
             loads[0].wait()
             loads[1].wait()
@@ -232,12 +267,12 @@
                 .reshape(2, 2, capacity, tile)
             )
 
-        over_width(out)
-        part_copy(source).start()
+        for i in range(PARTS):
+            over_width(i, out)
+            part_copy(source, i).start()
 
     def finish(step):
         source = order(step)
-        part_copy(source).wait_recv()
 
         def add(span):
             total = part[source, core, :, :, span].astype(jnp.float32) + part_in[source, :, :, span].astype(
@@ -245,12 +280,13 @@
             )
             done[source, :, :, span] = total.astype(jnp.bfloat16)
 
-        over_width(add)
-        done_copy(source).start()
+        for i in range(PARTS):
+            part_copy(source, i).wait_recv()
+            over_width(i, add)
+            done_copy(source, i).start()
 
     def combine(step):
         source = order(step)
-        done_copy(source).wait_recv()
         lane = lax.broadcasted_iota(jnp.int32, (tok_count, capacity), 1).astype(jnp.float32)
 
         def column(row):
@@ -267,23 +303,25 @@
             ) + share_other * jnp.dot(spread_other, done_in[source, :, span], preferred_element_type=jnp.float32)
             back[source, :, span] = total.astype(jnp.bfloat16)
 
-        over_width(merge)
-        if step:
-            back_copy(source).start()
+        for i in range(PARTS):
+            done_copy(source, i).wait_recv()
+            over_width(i, merge)
+            if step:
+                back_copy(source, i).start()
 
     for tick in range(line + 2):
         if tick < line:
             dispatch(tick)
         if 0 <= tick - 1 < line:
             compute(tick - 1)
-        if tick < line:
-            forward(tick)
-        if 0 <= tick - 1 < line:
+        if tick == line:
             finish(tick - 1)
         if 0 <= tick - 2 < line:
             combine(tick - 2)
-    for step in range(1, line):
-        back_arrival(order(step)).wait_recv()
+        if tick < line:
+            forward(tick)
+        if 0 <= tick - 1 < line - 1:
+            finish(tick - 1)
 
     def gather(span):
         total = back[z, :, span].astype(jnp.float32)
@@ -291,18 +329,23 @@
             total = total + back_in[order(step), :, span].astype(jnp.float32)
         out_ref[:, span] = total.astype(jnp.bfloat16)
 
-    over_width(gather)
+    for i in range(PARTS):
+        for step in range(1, line):
+            back_arrival(order(step), i).wait_recv()
+        over_width(i, gather)
     for step in range(line):
         source = order(step)
-        hops(source, lambda copy: copy.wait_send())
         if step:
             meta_copy(step).wait_send()
-            back_copy(source).wait_send()
-        cross_copy(source).wait_send()
-        for column in range(2):
-            pair_copy(source, column).wait_send()
-        part_copy(source).wait_send()
-        done_copy(source).wait_send()
+        for i in range(PARTS):
+            hops(source, i, lambda copy: copy.wait_send())
+            if step:
+                back_copy(source, i).wait_send()
+            cross_copy(source, i).wait_send()
+            for column in range(2):
+                pair_move(source, core, column, i).wait_send()
+            part_copy(source, i).wait_send()
+            done_copy(source, i).wait_send()
 
 
 def fused(line, tokens, norm_gain, expert_ids, route_weights, gate_proj, linear_proj, down_proj):
@@ -334,13 +377,13 @@
             pltpu.VMEM((line, tok_count, width), wide),
             pltpu.VMEM((line, tok_count, width), wide),
             dma((3,)),
-            dma((line, 2)), dma((line,)),
+            dma((line, PARTS, 2)), dma((line, PARTS)),
             dma((line,)), dma((line,)),
-            dma((line,)), dma((line,)),
-            dma((line, 2)), dma((line, 2)),
-            dma((line,)), dma((line,)),
-            dma((line,)), dma((line,)),
-            dma((line,)), dma((line,)),
+            dma((line, PARTS)), dma((line, PARTS)),
+            dma((line, 2, PARTS)), dma((line, 2, PARTS)),
+            dma((line, PARTS)), dma((line, PARTS)),
+            dma((line, PARTS)), dma((line, PARTS)),
+            dma((line, PARTS)), dma((line, PARTS)),
         ],
         compiler_params=pltpu.CompilerParams(
             collective_id=0, has_side_effects=True, vmem_limit_bytes=60 * 1024 * 1024

time: 109 us -> 106 us (0.972); the launches traced: 107 us -> 105 us
  Pallas kernels: 105 us -> 103 us
    pallas_call x1, Pallas kernels: 105 us -> 103 us  [fused(): pl.pallas_call(functools.partial(kernel, line), out_shape=jax.ShapeDtypeS...]
where the time goes in v2:
time: 106 us; the launch traced here: 105 us
  Pallas kernels  103 us (97%)
  local copies, waits for them, and re-layouts  1.88 us (2%)
    pallas_call x1, Pallas kernels, fused(): pl.pallas_call(functools.partial(kernel, line), out_shape=jax.ShapeDtypeS...  103 us

profile of v2, /device:TPU:24, one launch (start us, length us, event | category | flops | bytes accessed | tf_op | source)
XLA Modules:
  0.0 105.2 jit_solution(16501359839159456994)
XLA Ops:
  0.0 103.3 %experts.1 = bf16[128,2048]{1,0:T(8,128)(2,1)} custom-call(s32[2,128]{1,0:T(2,128)} %bitcast.10, f32[2,128]{1,0:T(2,128)} %bitcast.11, f32[1,2048]{1,0:T(1,128)} %bitcast.9, bf16[128,2048]{1,0:T(8,128)(2,1)} %tokens_ref.1, bf16[2048,768]{1,0:T(8,128)(2,1)} %bitcast.6, bf16[2048,768]{1,0:T(8,128)(2,1)} %bitcast.7, bf16[768,2048]{1,0:T(8,128)(2,1)} %bitcast.8), custom_call_target="tpu_custom_call" | custom-call | tf_op jit(solution)/shard_map/experts/pallas_call | solution.py:359
  103.3 1.9 %copy.9 = bf16[128,2048]{1,0:T(8,128)(2,1)} copy(bf16[128,2048]{1,0:T(8,128)(2,1)} %experts.1) | data formatting | bytes 1048576

commit v3 on v2

--- a/solution.py
+++ b/solution.py
@@ -50,9 +50,9 @@
 
 def kernel(
     line, ids_ref, weights_ref, gain_ref, tokens_ref, gate_hbm, linear_hbm, down_hbm, out_ref,
-    gate, linear, down, tok, meta, rows, cross, hidden, part, part_in, done, done_in, back, back_in,
+    gate, linear, down, tok, meta, rows, cross, hidden, part, part_in, done, back_in, total,
     load_sem, tok_send, tok_recv, meta_send, meta_recv, cross_send, cross_recv, pair_send, pair_recv,
-    part_send, part_recv, done_send, done_recv, back_send, back_recv,
+    part_send, part_recv, back_send, back_recv,
 ):
     ep, core = lax.axis_index("ep"), lax.axis_index("tp")
     z, y = ep // 2, ep % 2
@@ -81,9 +81,8 @@
     for load in loads:
         load.start()
     barrier = pltpu.get_barrier_semaphore()
-    for step in range(1, line):
-        pl.semaphore_signal(barrier, 1, device_id=at_z((z + step) % line), device_id_type=MESH)
-    pl.semaphore_signal(barrier, 1, device_id=at_y, device_id_type=MESH)
+    for step in range(1, experts):
+        pl.semaphore_signal(barrier, 1, device_id={"ep": (ep + step) % experts}, device_id_type=MESH)
     pl.semaphore_signal(barrier, 1, device_id=at_core, device_id_type=MESH)
 
     def normalize(i, _):
@@ -108,7 +107,7 @@
     slots = jnp.dot(chosen.astype(jnp.bfloat16), before, preferred_element_type=jnp.float32)
     meta[z, 0:experts, :] = jnp.where(chosen > 0.5, slots, -1.0)
     meta[z, experts : 2 * experts, :] = share
-    pl.semaphore_wait(barrier, line + 1)
+    pl.semaphore_wait(barrier, experts)
 
     def meta_copy(step):
         return remote(meta.at[z], meta.at[z], meta_send.at[step], meta_recv.at[z], at_z((z + step) % line))
@@ -164,22 +163,16 @@
             part_send.at[source, i], part_recv.at[source, i], at_core,
         )
 
-    def done_copy(source, i):
-        return remote(
-            done.at[source, 1 - y, :, cols[i]], done_in.at[source, :, cols[i]],
-            done_send.at[source, i], done_recv.at[source, i], at_y,
-        )
-
-    def back_copy(source, i):
-        return remote(
-            back.at[source, :, cols[i]], back_in.at[z, :, cols[i]],
-            back_send.at[source, i], back_recv.at[z, i], at_z(source),
-        )
-
-    def back_arrival(source, i):
-        return remote(
-            back.at[source, :, cols[i]], back_in.at[source, :, cols[i]],
-            back_send.at[source, i], back_recv.at[source, i], at_z(source),
+    def back_copy(source, column, i):
+        return remote(
+            done.at[source, column, :, cols[i]], back_in.at[z, y, :, cols[i]],
+            back_send.at[source, column, i], back_recv.at[z, y, i], {"ep": source * 2 + column},
+        )
+
+    def back_arrival(source, column, i):
+        return remote(
+            done.at[source, column, :, cols[i]], back_in.at[source, column, :, cols[i]],
+            back_send.at[source, column, i], back_recv.at[source, column, i], {"ep": source * 2 + column},
         )
 
     tile = 512
@@ -275,77 +268,69 @@
         source = order(step)
 
         def add(span):
-            total = part[source, core, :, :, span].astype(jnp.float32) + part_in[source, :, :, span].astype(
+            whole = part[source, core, :, :, span].astype(jnp.float32) + part_in[source, :, :, span].astype(
                 jnp.float32
             )
-            done[source, :, :, span] = total.astype(jnp.bfloat16)
+            done[source, :, :, span] = whole.astype(jnp.bfloat16)
 
         for i in range(PARTS):
             part_copy(source, i).wait_recv()
             over_width(i, add)
-            done_copy(source, i).start()
-
-    def combine(step):
-        source = order(step)
+            back_copy(source, 1 - y, i).start()
+            if step:
+                back_copy(source, y, i).start()
+
+    def gather(step, other):
+        source, column = order(step), 1 - y if other else y
+        expert = source * 2 + column
         lane = lax.broadcasted_iota(jnp.int32, (tok_count, capacity), 1).astype(jnp.float32)
 
-        def column(row):
-            return jnp.sum(jnp.where(eye, meta[source, pl.ds(row, 1), :], 0.0), axis=1, keepdims=True)
-
-        mine, other = z * 2 + y, z * 2 + 1 - y
-        spread_mine = (column(mine) == lane).astype(jnp.bfloat16)
-        spread_other = (column(other) == lane).astype(jnp.bfloat16)
-        share_mine, share_other = column(experts + mine), column(experts + other)
+        def upright(row):
+            return jnp.sum(jnp.where(eye, meta[z, pl.ds(row, 1), :], 0.0), axis=1, keepdims=True)
+
+        spread = (upright(expert) == lane).astype(jnp.bfloat16)
+        share_here = upright(experts + expert)
+        own = step == 0 and not other
 
         def merge(span):
-            total = share_mine * jnp.dot(
-                spread_mine, done[source, y, :, span], preferred_element_type=jnp.float32
-            ) + share_other * jnp.dot(spread_other, done_in[source, :, span], preferred_element_type=jnp.float32)
-            back[source, :, span] = total.astype(jnp.bfloat16)
-
-        for i in range(PARTS):
-            done_copy(source, i).wait_recv()
+            block = done[source, column, :, span] if own else back_in[source, column, :, span]
+            term = share_here * jnp.dot(spread, block, preferred_element_type=jnp.float32)
+            if own:
+                total[:, span] = term
+            elif step == line - 1 and other:
+                out_ref[:, span] = (total[:, span] + term).astype(jnp.bfloat16)
+            else:
+                total[:, span] = total[:, span] + term
+
+        for i in range(PARTS):
+            if not own:
+                back_arrival(source, column, i).wait_recv()
             over_width(i, merge)
-            if step:
-                back_copy(source, i).start()
-
-    for tick in range(line + 2):
+
+    for tick in range(line + 1):
         if tick < line:
             dispatch(tick)
-        if 0 <= tick - 1 < line:
+        if tick:
             compute(tick - 1)
-        if tick == line:
             finish(tick - 1)
-        if 0 <= tick - 2 < line:
-            combine(tick - 2)
         if tick < line:
             forward(tick)
-        if 0 <= tick - 1 < line - 1:
-            finish(tick - 1)
-
-    def gather(span):
-        total = back[z, :, span].astype(jnp.float32)
-        for step in range(1, line):
-            total = total + back_in[order(step), :, span].astype(jnp.float32)
-        out_ref[:, span] = total.astype(jnp.bfloat16)
-
-    for i in range(PARTS):
-        for step in range(1, line):
-            back_arrival(order(step), i).wait_recv()
-        over_width(i, gather)
+    for step in range(line):
+        gather(step, False)
+        gather(step, True)
     for step in range(line):
         source = order(step)
         if step:
             meta_copy(step).wait_send()
         for i in range(PARTS):
             hops(source, i, lambda copy: copy.wait_send())
+            back_copy(source, 1 - y, i).wait_send()
             if step:
-                back_copy(source, i).wait_send()
+                back_copy(source, y, i).wait_send()
             cross_copy(source, i).wait_send()
             for column in range(2):
                 pair_move(source, core, column, i).wait_send()
             part_copy(source, i).wait_send()
-            done_copy(source, i).wait_send()
 
 
 def fused(line, tokens, norm_gain, expert_ids, route_weights, gate_proj, linear_proj, down_proj):
@@ -373,17 +358,15 @@
             pltpu.VMEM((line, 2, 2, capacity, width), wide),
             pltpu.VMEM((line, 2, capacity, width), wide),
             pltpu.VMEM((line, 2, capacity, width), wide),
-            pltpu.VMEM((line, capacity, width), wide),
-            pltpu.VMEM((line, tok_count, width), wide),
-            pltpu.VMEM((line, tok_count, width), wide),
+            pltpu.VMEM((line, 2, capacity, width), wide),
+            pltpu.VMEM((tok_count, width), jnp.float32),
             dma((3,)),
             dma((line, PARTS, 2)), dma((line, PARTS)),
             dma((line,)), dma((line,)),
             dma((line, PARTS)), dma((line, PARTS)),
             dma((line, 2, PARTS)), dma((line, 2, PARTS)),
             dma((line, PARTS)), dma((line, PARTS)),
-            dma((line, PARTS)), dma((line, PARTS)),
-            dma((line, PARTS)), dma((line, PARTS)),
+            dma((line, 2, PARTS)), dma((line, 2, PARTS)),
         ],
         compiler_params=pltpu.CompilerParams(
             collective_id=0, has_side_effects=True, vmem_limit_bytes=60 * 1024 * 1024

time: 106 us -> 96.3 us (0.908)
  Pallas kernels: 103 us -> 94.3 us
    pallas_call x1, Pallas kernels: 103 us -> 94.3 us  [fused(): pl.pallas_call(functools.partial(kernel, line), out_shape=jax.ShapeDtypeS...]
where the time goes in v3:
time: 96.3 us; the launch traced here: 96.1 us
  Pallas kernels  94.3 us (98%)
  local copies, waits for them, and re-layouts  1.88 us (2%)
    pallas_call x1, Pallas kernels, fused(): pl.pallas_call(functools.partial(kernel, line), out_shape=jax.ShapeDtypeS...  94.3 us

profile of v3, /device:TPU:24, one launch (start us, length us, event | category | flops | bytes accessed | tf_op | source)
XLA Modules:
  0.0 96.1 jit_solution(6821109383793381782)
XLA Ops:
  0.0 94.3 %experts.1 = bf16[128,2048]{1,0:T(8,128)(2,1)} custom-call(s32[2,128]{1,0:T(2,128)} %bitcast.10, f32[2,128]{1,0:T(2,128)} %bitcast.11, f32[1,2048]{1,0:T(1,128)} %bitcast.9, bf16[128,2048]{1,0:T(8,128)(2,1)} %tokens_ref.1, bf16[2048,768]{1,0:T(8,128)(2,1)} %bitcast.6, bf16[2048,768]{1,0:T(8,128)(2,1)} %bitcast.7, bf16[768,2048]{1,0:T(8,128)(2,1)} %bitcast.8), custom_call_target="tpu_custom_call" | custom-call | tf_op jit(solution)/shard_map/experts/pallas_call | solution.py:344
  94.3 1.9 %copy.9 = bf16[128,2048]{1,0:T(8,128)(2,1)} copy(bf16[128,2048]{1,0:T(8,128)(2,1)} %experts.1) | data formatting | bytes 1048576

commit v4 on v3

--- a/solution.py
+++ b/solution.py
@@ -121,7 +121,7 @@
     def order(step):
         found = z
         for place in range(line):
-            nearest = sorted(range(line), key=lambda other: (abs(other - place), other))
+            nearest = sorted(range(line), key=lambda other: (abs(other - place), abs(2 * other - line + 1)))
             found = jnp.where(z == place, nearest[step], found)
         return found if step else z
 

time: 96.3 us -> 96.5 us (level)
  no operation moved by 1% of the time
where the time goes in v4:
time: 96.5 us; the launch traced here: 96.4 us
  Pallas kernels  94.5 us (98%)
  local copies, waits for them, and re-layouts  1.88 us (2%)
    pallas_call x1, Pallas kernels, fused(): pl.pallas_call(functools.partial(kernel, line), out_shape=jax.ShapeDtypeS...  94.5 us

profile of v4, /device:TPU:24, one launch (start us, length us, event | category | flops | bytes accessed | tf_op | source)
XLA Modules:
  0.0 96.4 jit_solution(1378453282618608294)
XLA Ops:
  0.0 94.5 %experts.1 = bf16[128,2048]{1,0:T(8,128)(2,1)} custom-call(s32[2,128]{1,0:T(2,128)} %bitcast.10, f32[2,128]{1,0:T(2,128)} %bitcast.11, f32[1,2048]{1,0:T(1,128)} %bitcast.9, bf16[128,2048]{1,0:T(8,128)(2,1)} %tokens_ref.1, bf16[2048,768]{1,0:T(8,128)(2,1)} %bitcast.6, bf16[2048,768]{1,0:T(8,128)(2,1)} %bitcast.7, bf16[768,2048]{1,0:T(8,128)(2,1)} %bitcast.8), custom_call_target="tpu_custom_call" | custom-call | tf_op jit(solution)/shard_map/experts/pallas_call | solution.py:344
  94.5 1.9 %copy.9 = bf16[128,2048]{1,0:T(8,128)(2,1)} copy(bf16[128,2048]{1,0:T(8,128)(2,1)} %experts.1) | data formatting | bytes 1048576
